TPU v7x, 32 devices: a whole 2x2x4 slice. The times are simulated.
32 devices in a mesh: grp: 2 (over y), fs: 4 (over z), tp: 4 (over x, core).
Axes of the slice: x: 2, y: 2, z: 4, core: 2. Of those that a mesh axis runs over, the one named last changes fastest.
Arguments:
- tokens: bfloat16 [8192, 2048], P(('grp', 'fs')), parts along dimension 0, may hold values from -6 to 6
- mixer_gain: float32 [2048], replicated, may hold values from 0.1 to 1.9
- outer_weight: float32 [2048, 2048], P('fs', 'tp'), may hold values from -0.125 to 0.125
- inner_weight: float32 [2048, 2048], P('fs', 'tp'), may hold values from -0.125 to 0.125
- value_weight: float32 [2048, 2048], P('fs', 'tp'), may hold values from -0.125 to 0.125
- filter_taps: float32 [3, 2048], P(None, 'tp'), may hold values from -3.5 to 3.5
- mixer_weight: float32 [2048, 2048], P('tp', 'fs'), may hold values from -0.125 to 0.125
- outer_scale: float32 [4, 512], P('tp', 'fs'), may hold values from 0.5 to 2
- inner_scale: float32 [4, 512], P('tp', 'fs'), may hold values from 0.5 to 2
- value_scale: float32 [4, 512], P('tp', 'fs'), may hold values from 0.5 to 2
- mixer_scale: float32 [1, 2048], P(None, 'fs'), may hold values from 0.5 to 2
Outputs:
- layer_out: bfloat16 [8192, 2048], P(('grp', 'fs', 'tp')), parts along dimension 0
There are 2 independent parts, one for each index of `grp`. A program takes and returns all parts, laid end to end along the dimension named above; an argument that names none is the same for every part. Nothing has to cross between parts.
All inputs are finite; a program needn't handle non-finite values.
Results may differ from a plain program's by a relative error of at most 0.014.
Values may be sent and summed in bfloat16 or wider, within the bound.
A program may use at most 64 MiB of HBM per device.

v0:
```python
import jax
import jax.numpy as jnp
from jax import lax
from jax.sharding import PartitionSpec as P

EPS = 1e-06


def normed(rows, gain):
    values = rows.astype(jnp.float32)
    inverse = lax.rsqrt(jnp.mean(values * values, axis=-1, keepdims=True) + EPS)
    return (values * inverse * gain).astype(jnp.bfloat16)


def rounded(values):
    return lax.optimization_barrier(values.astype(jnp.bfloat16)).astype(jnp.float32)


def add_rows(left, piece):
    return jnp.dot(left, piece, preferred_element_type=jnp.float32)


def per_device(
    tokens,
    mixer_gain,
    outer_weight,
    inner_weight,
    value_weight,
    filter_taps,
    mixer_weight,
    outer_scale,
    inner_scale,
    value_scale,
    mixer_scale,
):
    gathered = (
        lax.all_gather(outer_scale, "fs", axis=1, tiled=True),
        lax.all_gather(inner_scale, "fs", axis=1, tiled=True),
        lax.all_gather(value_scale, "fs", axis=1, tiled=True),
        lax.all_gather(mixer_scale, "fs", axis=1, tiled=True),
    )
    outer_col, inner_col, value_col, mixer_col = [piece.reshape(-1) for piece in gathered]
    seq_rows = tokens.shape[0]
    normal_rows = normed(tokens, mixer_gain)

    def fold_one(piece):
        return add_rows(normal_rows, piece)

    outer_sum = fold_one(
        lax.all_gather(outer_weight.astype(jnp.bfloat16), "fs", axis=0, tiled=True)
    )
    inner_sum = fold_one(
        lax.all_gather(inner_weight.astype(jnp.bfloat16), "fs", axis=0, tiled=True)
    )
    value_sum = fold_one(
        lax.all_gather(value_weight.astype(jnp.bfloat16), "fs", axis=0, tiled=True)
    )
    outer = rounded(outer_sum * outer_col)
    inner = rounded(inner_sum * inner_col)
    value = rounded(value_sum * value_col)
    padded = jnp.pad(inner * value, ((2, 0), (0, 0)))
    filtered = (
        filter_taps[0] * padded[0:seq_rows]
        + filter_taps[1] * padded[1 : seq_rows + 1]
        + filter_taps[2] * padded[2:]
    )
    gated = (outer * filtered).astype(jnp.bfloat16)
    mixer_full = lax.all_gather(mixer_weight.astype(jnp.bfloat16), "fs", axis=1, tiled=True)
    return lax.psum_scatter(
        (jnp.dot(gated, mixer_full, preferred_element_type=jnp.float32) * mixer_col).astype(
            jnp.bfloat16
        ),
        "tp",
        scatter_dimension=0,
        tiled=True,
    )


def solution(mesh):
    in_specs = (
        P(("grp", "fs"), None),
        P(),
        P("fs", "tp"),
        P("fs", "tp"),
        P("fs", "tp"),
        P(None, "tp"),
        P("tp", "fs"),
        P("tp", "fs"),
        P("tp", "fs"),
        P("tp", "fs"),
        P(None, "fs"),
    )
    out_specs = P(("grp", "fs", "tp"), None)
    return jax.shard_map(
        per_device, mesh=mesh, in_specs=in_specs, out_specs=out_specs, check_vma=False
    )
```

profile of v0, /device:TPU:0, one launch (start us, length us, event | category | flops | bytes accessed | tf_op | source)
XLA Modules:
  0.0 252.3 jit_solution(7031129598482165264)
XLA Ops:
  6.5 2.2 convert_element_type.46
  8.8 0.0 all-gather.5.cloned.1.call-update
  8.8 0.0 all-gather.7.cloned.1.call-start
  8.9 0.9 convert_element_type.49
  9.8 0.0 all-gather.9.cloned.1.call-start
  9.9 0.9 convert_element_type.52
  10.8 0.0 all-gather.11.cloned.1.call-start
  10.8 0.9 convert_element_type.56
  11.8 0.0 reduce-scatter.2.cloned.1.call-start
  11.8 12.7 %all_gather.25 = f32[1,512]{1,0:T(1,128)S(1)} all-gather(f32[1,128]{1,0:T(1,128)S(1)} %copy-done.5), channel_id=1, replica_groups=mesh['grp'=2,'fs'=4,'tp'=4] {'fs'}, dimensions={1}, use_global_device_ids=true | all-gather | bytes 2560 | tf_op jit(solution)/shard_map/all_gather | solution.py:37
  24.6 7.9 %all_gather.27 = f32[1,512]{1,0:T(1,128)S(1)} all-gather(f32[1,128]{1,0:T(1,128)S(1)} %copy-done.6), channel_id=1, replica_groups=mesh['grp'=2,'fs'=4,'tp'=4] {'fs'}, dimensions={1}, use_global_device_ids=true | all-gather | bytes 2560 | tf_op jit(solution)/shard_map/all_gather | solution.py:38
  32.5 11.0 %all_gather.29 = f32[1,512]{1,0:T(1,128)S(1)} all-gather(f32[1,128]{1,0:T(1,128)S(1)} %copy-done.7), channel_id=1, replica_groups=mesh['grp'=2,'fs'=4,'tp'=4] {'fs'}, dimensions={1}, use_global_device_ids=true | all-gather | bytes 2560 | tf_op jit(solution)/shard_map/all_gather | solution.py:39
  43.5 12.6 %all_gather.31 = f32[1,2048]{1,0:T(1,128)S(1)} all-gather(f32[1,512]{1,0:T(1,128)S(1)} %copy-done.4), channel_id=1, replica_groups=mesh['grp'=2,'fs'=4,'tp'=4] {'fs'}, dimensions={1}, use_global_device_ids=true | all-gather | bytes 10240 | tf_op jit(solution)/shard_map/all_gather | solution.py:40
  56.2 3.1 %fusion = f32[1024]{0:T(1024)S(1)} fusion(bf16[1024,2048]{1,0:T(8,128)(2,1)} %param.11), kind=kLoop, calls=%fused_computation.2 | loop fusion | flops 6290432 | bytes 4198400 | tf_op jit(solution)/shard_map/reduce_sum | solution.py:11
  59.3 0.0 all-gather.5.cloned.1.call-done
  59.4 6.2 %multiply_convert_fusion.4 = bf16[1024,512]{1,0:T(8,128)(2,1)} fusion(bf16[2048,512]{1,0:T(8,128)(2,1)} %all-gather.5.cloned.1.call-done, f32[512]{0:T(512)S(1)} %bitcast.14, bf16[1024,2048]{1,0:T(8,128)(2,1)} %param.11, f32[2048]{0:T(1024)S(1)} %copy-done.8, f32[1024]{0:T(1024)S(1)} %add_rsqrt_fusion), kind=kOutput, calls=%fused_computation.10 | convolution fusion | flops 2156920832 | bytes 7354368 | tf_op jit(solution)/shard_map/dot_general | solution.py:20
  65.6 38.0 %all-gather.7.cloned.1.call-done = bf16[2048,512]{1,0:T(8,128)(2,1)} async-done(((bf16[512,512]{1,0:T(8,128)(2,1)}), bf16[2048,512]{1,0:T(8,128)(2,1)}) %all-gather.7.cloned.1.call-update) | async-done | bytes 2097168 | tf_op jit(solution)/shard_map/all_gather | solution.py:53
  103.6 5.2 %multiply_convert_fusion.3 = bf16[1024,512]{1,0:T(8,128)(2,1)S(1)} fusion(bf16[2048,512]{1,0:T(8,128)(2,1)} %all-gather.7.cloned.1.call-done, f32[512]{0:T(512)S(1)} %bitcast.13, bf16[1024,2048]{1,0:T(8,128)(2,1)} %param.11, f32[2048]{0:T(1024)S(1)} %copy-done.8, f32[1024]{0:T(1024)S(1)} %add_rsqrt_fusion), kind=kOutput, calls=%fused_computation.9 | convolution fusion | flops 2156920832 | bytes 7354368 | tf_op jit(solution)/shard_map/dot_general | solution.py:20
  108.8 40.8 %all-gather.9.cloned.1.call-done = bf16[2048,512]{1,0:T(8,128)(2,1)} async-done(((bf16[512,512]{1,0:T(8,128)(2,1)}), bf16[2048,512]{1,0:T(8,128)(2,1)}) %all-gather.9.cloned.1.call-update) | async-done | bytes 2097168 | tf_op jit(solution)/shard_map/all_gather | solution.py:56
  149.7 5.2 %multiply_convert_fusion.2 = bf16[1024,512]{1,0:T(8,128)(2,1)S(1)} fusion(bf16[2048,512]{1,0:T(8,128)(2,1)} %all-gather.9.cloned.1.call-done, f32[512]{0:T(512)S(1)} %bitcast.12, bf16[1024,2048]{1,0:T(8,128)(2,1)} %param.11, f32[2048]{0:T(1024)S(1)} %copy-done.8, f32[1024]{0:T(1024)S(1)} %add_rsqrt_fusion), kind=kOutput, calls=%fused_computation.8 | convolution fusion | flops 2156920832 | bytes 7354368 | tf_op jit(solution)/shard_map/dot_general | solution.py:20
  154.9 0.3 convert_multiply_fusion.2
  155.2 40.4 %all-gather.11.cloned.1.call-done = bf16[512,2048]{1,0:T(8,128)(2,1)} async-done(((bf16[512,512]{1,0:T(8,128)(2,1)}), bf16[512,2048]{1,0:T(8,128)(2,1)}) %all-gather.11.cloned.1.call-update) | async-done | bytes 2097168 | tf_op jit(solution)/shard_map/all_gather | solution.py:68
  195.6 6.6 %multiply_convert_fusion = bf16[1024,2048]{1,0:T(8,128)(2,1)} fusion(bf16[512,2048]{1,0:T(8,128)(2,1)} %all-gather.11.cloned.1.call-done, f32[2048]{0:T(1024)S(1)} %bitcast.11, f32[1024,512]{1,0:T(8,128)S(1)} %convert_multiply_fusion.2, bf16[1024,512]{1,0:T(8,128)(2,1)} %multiply_convert_fusion.4, f32[512]{0:T(512)S(1)} %bitcast.16, f32[512]{0:T(512)S(1)} %bitcast.17, ...), kind=kOutput, calls=%fused_computation.5 | convolution fusion | flops 2155872256 | bytes 9451520 | tf_op jit(solution)/shard_map/dot_general | solution.py:70
  202.2 43.6 %reduce-scatter.2.cloned.1.call-done = bf16[256,2048]{1,0:T(8,128)(2,1)} async-done(((bf16[1024,2048]{1,0:T(8,128)(2,1)}), bf16[256,2048]{1,0:T(8,128)(2,1)}) %reduce-scatter.2.cloned.1.call-update) | async-done | bytes 1048592 | tf_op jit(solution)/shard_map/reduce_scatter | solution.py:69
  (25 shorter events, 0.1 us)
Async XLA Ops:
  6.5 2.3 copy-start
  6.5 3.3 %copy-start.1 = (f32[512,512]{1,0:T(8,128)S(1)}, f32[512,512]{1,0:T(8,128)}, u32[]{:S(2)}) copy-start(f32[512,512]{1,0:T(8,128)} %param.15) | copy-start | bytes 3145732
  6.5 52.8 %all-gather.5.cloned.1.call-start = ((), (), s32[]{:S(2)}) async-start(), calls=%async_computation.1 | async-start | bytes 2621440 | tf_op jit(solution)/shard_map/all_gather | solution.py:50
  8.8 2.0 copy-start.2
  8.8 94.8 %all-gather.7.cloned.1.call-start = ((), (), s32[]{:S(2)}) async-start(), calls=%async_computation.2 | async-start | bytes 2621440 | tf_op jit(solution)/shard_map/all_gather | solution.py:53
  9.8 2.1 copy-start.5
  9.8 14.8 %copy-start.6 = (f32[1,128]{1,0:T(1,128)S(1)}, f32[1,128]{1,0:T(1,128)}, u32[]{:S(2)}) copy-start(f32[1,128]{1,0:T(1,128)} %param.19) | copy-start | bytes 1540
  9.8 22.7 %copy-start.7 = (f32[1,128]{1,0:T(1,128)S(1)}, f32[1,128]{1,0:T(1,128)}, u32[]{:S(2)}) copy-start(f32[1,128]{1,0:T(1,128)} %param.20) | copy-start | bytes 1540
  9.8 33.7 %copy-start.4 = (f32[1,512]{1,0:T(1,128)S(1)}, f32[1,512]{1,0:T(1,128)}, u32[]{:S(2)}) copy-start(f32[1,512]{1,0:T(1,128)} %param.21) | copy-start | bytes 6148
  9.8 139.9 %all-gather.9.cloned.1.call-start = ((), (), s32[]{:S(2)}) async-start(), calls=%async_computation.3 | async-start | bytes 2621440 | tf_op jit(solution)/shard_map/all_gather | solution.py:56
  10.8 184.8 %all-gather.11.cloned.1.call-start = ((), (), s32[]{:S(2)}) async-start(), calls=%async_computation.4 | async-start | bytes 2621440 | tf_op jit(solution)/shard_map/all_gather | solution.py:68
  11.8 234.0 %reduce-scatter.2.cloned.1.call-start = ((), (), s32[]{:S(2)}) async-start(), calls=%async_computation.5 | async-start | bytes 5242880 | tf_op jit(solution)/shard_map/reduce_scatter | solution.py:69
  56.2 3.1 %copy-start.3 = (f32[3,512]{1,0:T(4,128)S(1)}, f32[3,512]{1,0:T(4,128)}, u32[]{:S(2)}) copy-start(f32[3,512]{1,0:T(4,128)} %param.16) | copy-start | bytes 18436
  56.2 3.2 %copy-start.8 = (f32[2048]{0:T(1024)S(1)}, f32[2048]{0:T(1024)}, u32[]{:S(2)}) copy-start(f32[2048]{0:T(1024)} %param.12) | copy-start | bytes 24580
Sparse Core Ops, SparseCore 0:
  8.9 48.5 all-gather.4
  59.1 44.4 all-gather.6
  105.2 44.4 all-gather.8
  151.1 44.4 all-gather.10
  202.3 43.3 reduce-scatter.1
where the time goes:
time: 252 us
  waiting for transfers between devices  163 us (65%)
  blocking collectives  44.3 us (18%)
  matrix products  23.3 us (9%)
  between operations  13.3 us (5%)
  other arithmetic  8.31 us (3%)
    reduce_scatter x1, waiting for transfers between devices, per_device(): lax.psum_scatter((jnp.dot(gated, mixer_full, preferred_element_type=jnp.f...  43.6 us
    all_gather x1, waiting for transfers between devices, per_device(): lax.all_gather(value_weight.astype(jnp.bfloat16), 'fs', axis=0, tiled=True)  40.8 us
    all_gather x1, waiting for transfers between devices, per_device(): lax.all_gather(mixer_weight.astype(jnp.bfloat16), 'fs', axis=1, tiled=True)  40.4 us
    all_gather x1, waiting for transfers between devices, per_device(): lax.all_gather(inner_weight.astype(jnp.bfloat16), 'fs', axis=0, tiled=True)  38 us
    dot_general x3, matrix products, add_rows(): return jnp.dot(left, piece, preferred_element_type=jnp.float32)  16.7 us
    all_gather x1, blocking collectives, per_device(): lax.all_gather(outer_scale, 'fs', axis=1, tiled=True)  12.7 us
    all_gather x1, blocking collectives, per_device(): lax.all_gather(mixer_scale, 'fs', axis=1, tiled=True)  12.6 us
    all_gather x1, blocking collectives, per_device(): lax.all_gather(value_scale, 'fs', axis=1, tiled=True)  11 us
  transfers between devices with their start and end apart: 5, of which 4 were waited for; matrix products, arithmetic and copies ran while one was open for 9% of the time, Pallas kernels for 0%

commit v1 on v0

--- a/solution.py
+++ b/solution.py
@@ -4,6 +4,13 @@
 from jax.sharding import PartitionSpec as P
 
 EPS = 1e-06
+
+
+def swapped_in(x, axis, dim):
+    n_dev = lax.axis_size(axis)
+    pieces = jnp.stack([x for _ in range(n_dev)])
+    pieces = lax.all_to_all(pieces, axis, split_axis=0, concat_axis=0)
+    return jnp.concatenate(pieces, axis=dim)
 
 
 def normed(rows, gain):
@@ -49,9 +56,7 @@
     outer_sum = fold_one(
         lax.all_gather(outer_weight.astype(jnp.bfloat16), "fs", axis=0, tiled=True)
     )
-    inner_sum = fold_one(
-        lax.all_gather(inner_weight.astype(jnp.bfloat16), "fs", axis=0, tiled=True)
-    )
+    inner_sum = fold_one(swapped_in(inner_weight.astype(jnp.bfloat16), "fs", 0))
     value_sum = fold_one(
         lax.all_gather(value_weight.astype(jnp.bfloat16), "fs", axis=0, tiled=True)
     )

time: 252 us -> 246 us (0.976)
  waiting for transfers between devices: 163 us -> 81.4 us
  blocking collectives: 44.3 us -> 113 us
  starting transfers between devices: 0.17 us -> 6.6 us
    all_gather x1, blocking collectives: 12.7 us -> 71.6 us  [per_device(): lax.all_gather(outer_scale, 'fs', axis=1, tiled=True)]
    all_gather x1, waiting for transfers between devices: 40.8 us -> 1.99 us  [per_device(): lax.all_gather(value_weight.astype(jnp.bfloat16), 'fs', axis=0, tiled=True)]
    all_gather x1 -> x0, waiting for transfers between devices: 38 us -> none  [per_device(): lax.all_gather(inner_weight.astype(jnp.bfloat16), 'fs', axis=0, tiled=True)]
    all_gather x1, blocking collectives: 7.94 us -> 20.4 us  [per_device(): lax.all_gather(inner_scale, 'fs', axis=1, tiled=True)]
    all_to_all x0 -> x1, starting transfers between devices: none -> 6.48 us  [swapped_in(): pieces = lax.all_to_all(pieces, axis, split_axis=0, concat_axis=0)]
    all_gather x1, waiting for transfers between devices: 40.4 us -> 35.8 us  [per_device(): lax.all_gather(mixer_weight.astype(jnp.bfloat16), 'fs', axis=1, tiled=True)]
    all_gather x1, blocking collectives: 11 us -> 8.04 us  [per_device(): lax.all_gather(value_scale, 'fs', axis=1, tiled=True)]
  transfers between devices with their start and end apart: 5 -> 5, of which waited for: 4 -> 3; matrix products, arithmetic and copies ran while one was open for 9% -> 9% of each run, Pallas kernels for 0% -> 0%
where the time goes in v1:
time: 246 us
  blocking collectives  113 us (46%)
  waiting for transfers between devices  81.4 us (33%)
  matrix products  22.8 us (9%)
  between operations  13.2 us (5%)
  other arithmetic  7.53 us (3%)
  starting transfers between devices  6.6 us (3%)
    all_gather x1, blocking collectives, per_device(): lax.all_gather(outer_scale, 'fs', axis=1, tiled=True)  71.6 us
    reduce_scatter x1, waiting for transfers between devices, per_device(): lax.psum_scatter((jnp.dot(gated, mixer_full, preferred_element_type=jnp.f...  43.5 us
    all_gather x1, waiting for transfers between devices, per_device(): lax.all_gather(mixer_weight.astype(jnp.bfloat16), 'fs', axis=1, tiled=True)  35.8 us
    all_gather x1, blocking collectives, per_device(): lax.all_gather(inner_scale, 'fs', axis=1, tiled=True)  20.4 us
    dot_general x3, matrix products, add_rows(): return jnp.dot(left, piece, preferred_element_type=jnp.float32)  16.2 us
    all_gather x1, blocking collectives, per_device(): lax.all_gather(mixer_scale, 'fs', axis=1, tiled=True)  12.6 us
    all_gather x1, blocking collectives, per_device(): lax.all_gather(value_scale, 'fs', axis=1, tiled=True)  8.04 us
    dot_general x1, matrix products, per_device(): jnp.dot(gated, mixer_full, preferred_element_type=jnp.float32) * mixer_col  6.6 us
  transfers between devices with their start and end apart: 5, of which 3 were waited for; matrix products, arithmetic and copies ran while one was open for 9% of the time, Pallas kernels for 0%

profile of v1, /device:TPU:0, one launch (start us, length us, event | category | flops | bytes accessed | tf_op | source)
XLA Modules:
  0.0 245.8 jit_solution(1600985459476163786)
XLA Ops:
  6.5 2.2 convert_element_type.46
  8.8 0.0 all-gather.4.cloned.1.call-update
  8.8 0.0 all-gather.6.cloned.1.call-start
  8.9 0.9 convert_element_type.52
  9.8 0.1 convert_element_type.49
  9.8 1.5 stack.2
  11.4 6.5 %all-to-all-start = ((bf16[4,512,512]{2,1,0:T(8,128)(2,1)}), bf16[4,512,512]{2,1,0:T(8,128)(2,1)S(1)}, u32[]{:S(2)}, u32[]{:S(2)}) async-start(bf16[4,512,512]{2,1,0:T(8,128)(2,1)} %stack.2), calls=%async_computation | async-start | bytes 4194304 | tf_op jit(solution)/shard_map/all_to_all | solution.py:12
  17.9 0.0 all-gather.8.cloned.1.call-start
  17.9 0.9 convert_element_type.56
  18.9 0.0 reduce-scatter.2.cloned.1.call-start
  18.9 71.6 %all_gather.22 = f32[1,512]{1,0:T(1,128)S(1)} all-gather(f32[1,128]{1,0:T(1,128)S(1)} %copy-done.5), channel_id=1, replica_groups=mesh['grp'=2,'fs'=4,'tp'=4] {'fs'}, dimensions={1}, use_global_device_ids=true | all-gather | bytes 2560 | tf_op jit(solution)/shard_map/all_gather | solution.py:44
  90.5 20.4 %all_gather.23 = f32[1,512]{1,0:T(1,128)S(1)} all-gather(f32[1,128]{1,0:T(1,128)S(1)} %copy-done.6), channel_id=1, replica_groups=mesh['grp'=2,'fs'=4,'tp'=4] {'fs'}, dimensions={1}, use_global_device_ids=true | all-gather | bytes 2560 | tf_op jit(solution)/shard_map/all_gather | solution.py:45
  110.9 8.0 %all_gather.25 = f32[1,512]{1,0:T(1,128)S(1)} all-gather(f32[1,128]{1,0:T(1,128)S(1)} %copy-done.7), channel_id=1, replica_groups=mesh['grp'=2,'fs'=4,'tp'=4] {'fs'}, dimensions={1}, use_global_device_ids=true | all-gather | bytes 2560 | tf_op jit(solution)/shard_map/all_gather | solution.py:46
  118.9 12.6 %all_gather.27 = f32[1,2048]{1,0:T(1,128)S(1)} all-gather(f32[1,512]{1,0:T(1,128)S(1)} %copy-done.4), channel_id=1, replica_groups=mesh['grp'=2,'fs'=4,'tp'=4] {'fs'}, dimensions={1}, use_global_device_ids=true | all-gather | bytes 10240 | tf_op jit(solution)/shard_map/all_gather | solution.py:47
  131.6 3.1 %fusion = f32[1024]{0:T(1024)S(1)} fusion(bf16[1024,2048]{1,0:T(8,128)(2,1)} %param.11), kind=kLoop, calls=%fused_computation.2 | loop fusion | flops 6290432 | bytes 4198400 | tf_op jit(solution)/shard_map/reduce_sum | solution.py:18
  134.8 0.0 all-gather.4.cloned.1.call-done
  134.8 6.2 %multiply_convert_fusion.4 = bf16[1024,512]{1,0:T(8,128)(2,1)} fusion(bf16[2048,512]{1,0:T(8,128)(2,1)} %all-gather.4.cloned.1.call-done, f32[512]{0:T(512)S(1)} %bitcast.16, bf16[1024,2048]{1,0:T(8,128)(2,1)} %param.11, f32[2048]{0:T(1024)S(1)} %copy-done.8, f32[1024]{0:T(1024)S(1)} %add_rsqrt_fusion), kind=kOutput, calls=%fused_computation.10 | convolution fusion | flops 2156920832 | bytes 7354368 | tf_op jit(solution)/shard_map/dot_general | solution.py:27
  141.0 2.0 all-gather.6.cloned.1.call-done
  143.0 5.3 %multiply_convert_fusion.2 = bf16[1024,512]{1,0:T(8,128)(2,1)S(1)} fusion(bf16[2048,512]{1,0:T(8,128)(2,1)} %all-gather.6.cloned.1.call-done, f32[512]{0:T(512)S(1)} %bitcast.15, bf16[1024,2048]{1,0:T(8,128)(2,1)} %param.11, f32[2048]{0:T(1024)S(1)} %copy-done.8, f32[1024]{0:T(1024)S(1)} %add_rsqrt_fusion), kind=kOutput, calls=%fused_computation.8 | convolution fusion | flops 2156920832 | bytes 7354368 | tf_op jit(solution)/shard_map/dot_general | solution.py:27
  148.3 4.7 %multiply_convert_fusion.3 = bf16[1024,512]{1,0:T(8,128)(2,1)S(1)} fusion(bf16[2048,512]{1,0:T(8,128)(2,1)S(1)} %bitcast.12, f32[512]{0:T(512)S(1)} %bitcast.14, bf16[1024,2048]{1,0:T(8,128)(2,1)} %param.11, f32[2048]{0:T(1024)S(1)} %copy-done.8, f32[1024]{0:T(1024)S(1)} %add_rsqrt_fusion), kind=kOutput, calls=%fused_computation.9 | convolution fusion | flops 2156920832 | bytes 7354368 | tf_op jit(solution)/shard_map/dot_general | solution.py:27
  153.0 0.3 convert_multiply_fusion.2
  153.3 35.8 %all-gather.8.cloned.1.call-done = bf16[512,2048]{1,0:T(8,128)(2,1)} async-done(((bf16[512,512]{1,0:T(8,128)(2,1)}), bf16[512,2048]{1,0:T(8,128)(2,1)}) %all-gather.8.cloned.1.call-update) | async-done | bytes 2097168 | tf_op jit(solution)/shard_map/all_gather | solution.py:73
  189.1 6.6 %multiply_convert_fusion = bf16[1024,2048]{1,0:T(8,128)(2,1)} fusion(bf16[512,2048]{1,0:T(8,128)(2,1)} %all-gather.8.cloned.1.call-done, f32[2048]{0:T(1024)S(1)} %bitcast.13, f32[1024,512]{1,0:T(8,128)S(1)} %convert_multiply_fusion.2, bf16[1024,512]{1,0:T(8,128)(2,1)} %multiply_convert_fusion.4, f32[512]{0:T(512)S(1)} %bitcast.18, f32[512]{0:T(512)S(1)} %bitcast.19, ...), kind=kOutput, calls=%fused_computation.5 | convolution fusion | flops 2155872256 | bytes 9451520 | tf_op jit(solution)/shard_map/dot_general | solution.py:75
  195.7 43.5 %reduce-scatter.2.cloned.1.call-done = bf16[256,2048]{1,0:T(8,128)(2,1)} async-done(((bf16[1024,2048]{1,0:T(8,128)(2,1)}), bf16[256,2048]{1,0:T(8,128)(2,1)}) %reduce-scatter.2.cloned.1.call-update) | async-done | bytes 1048592 | tf_op jit(solution)/shard_map/reduce_scatter | solution.py:74
  (25 shorter events, 0.1 us)
Async XLA Ops:
  6.5 2.3 copy-start
  6.5 3.2 %copy-start.1 = (f32[512,512]{1,0:T(8,128)S(1)}, f32[512,512]{1,0:T(8,128)}, u32[]{:S(2)}) copy-start(f32[512,512]{1,0:T(8,128)} %param.14) | copy-start | bytes 3145732
  6.5 128.2 %all-gather.4.cloned.1.call-start = ((), (), s32[]{:S(2)}) async-start(), calls=%async_computation.2 | async-start | bytes 2621440 | tf_op jit(solution)/shard_map/all_gather | solution.py:57
  8.8 134.2 %all-gather.6.cloned.1.call-start = ((), (), s32[]{:S(2)}) async-start(), calls=%async_computation.3 | async-start | bytes 2621440 | tf_op jit(solution)/shard_map/all_gather | solution.py:61
  11.4 6.6 %copy-start.2 = (f32[512,512]{1,0:T(8,128)S(1)}, f32[512,512]{1,0:T(8,128)}, u32[]{:S(2)}) copy-start(f32[512,512]{1,0:T(8,128)} %param.17) | copy-start | bytes 3145732
  11.4 136.9 %all-to-all-start = ((bf16[4,512,512]{2,1,0:T(8,128)(2,1)}), bf16[4,512,512]{2,1,0:T(8,128)(2,1)S(1)}, u32[]{:S(2)}, u32[]{:S(2)}) async-start(bf16[4,512,512]{2,1,0:T(8,128)(2,1)} %stack.2), calls=%async_computation | async-start | bytes 4194304 | tf_op jit(solution)/shard_map/all_to_all | solution.py:12
  17.8 1.1 copy-start.5
  17.8 72.7 %copy-start.6 = (f32[1,128]{1,0:T(1,128)S(1)}, f32[1,128]{1,0:T(1,128)}, u32[]{:S(2)}) copy-start(f32[1,128]{1,0:T(1,128)} %param.19) | copy-start | bytes 1540
  17.9 93.1 %copy-start.7 = (f32[1,128]{1,0:T(1,128)S(1)}, f32[1,128]{1,0:T(1,128)}, u32[]{:S(2)}) copy-start(f32[1,128]{1,0:T(1,128)} %param.20) | copy-start | bytes 1540
  17.9 101.1 %copy-start.4 = (f32[1,512]{1,0:T(1,128)S(1)}, f32[1,512]{1,0:T(1,128)}, u32[]{:S(2)}) copy-start(f32[1,512]{1,0:T(1,128)} %param.21) | copy-start | bytes 6148
  17.9 171.2 %all-gather.8.cloned.1.call-start = ((), (), s32[]{:S(2)}) async-start(), calls=%async_computation.4 | async-start | bytes 2621440 | tf_op jit(solution)/shard_map/all_gather | solution.py:73
  18.9 220.4 %reduce-scatter.2.cloned.1.call-start = ((), (), s32[]{:S(2)}) async-start(), calls=%async_computation.5 | async-start | bytes 5242880 | tf_op jit(solution)/shard_map/reduce_scatter | solution.py:74
  131.6 3.1 %copy-start.3 = (f32[3,512]{1,0:T(4,128)S(1)}, f32[3,512]{1,0:T(4,128)}, u32[]{:S(2)}) copy-start(f32[3,512]{1,0:T(4,128)} %param.16) | copy-start | bytes 18436
  131.6 3.2 %copy-start.8 = (f32[2048]{0:T(1024)S(1)}, f32[2048]{0:T(1024)}, u32[]{:S(2)}) copy-start(f32[2048]{0:T(1024)} %param.12) | copy-start | bytes 24580
Sparse Core Ops, SparseCore 0:
  8.9 86.5 all-gather.3
  97.0 45.9 all-gather.5
  144.6 44.4 all-gather.7
  195.8 43.3 reduce-scatter.1
